TPU v7x, 32 devices: a whole 2x2x4 slice. The times are simulated.
32 devices in a mesh: sp: 8 (over z, core), tp: 4 (over y, x).
Axes of the slice: x: 2, y: 2, z: 4, core: 2. Of those that a mesh axis runs over, the one named last changes fastest.
Arguments:
- residual: bfloat16 [2048, 2048], P('sp'), may hold values from -6 to 6
- queries: bfloat16 [2048, 16, 128], P('sp', 'tp'), may hold values from -256 to 256
- key_vectors: bfloat16 [2048, 16, 128], P('sp', 'tp'), may hold values from -5.3 to 5.3
- value_rows: bfloat16 [2048, 16, 128], P('sp', 'tp'), may hold values from -6 to 6
- head_lambda: float32 [16], P('tp'), may hold values from 0.3 to 0.8
- head_gain: float32 [128], replicated, may hold values from 0.1 to 1.9
- out_weight: bfloat16 [2048, 2048], P('tp'), may hold values from -0.125 to 0.125
- ffn_gain: float32 [2048], replicated, may hold values from 0.1 to 1.9
- expert_gate: bfloat16 [8, 2048, 4096], P('sp', None, 'tp'), may hold values from -0.125 to 0.125
- expert_up: bfloat16 [8, 2048, 4096], P('sp', None, 'tp'), may hold values from -0.125 to 0.125
- expert_down: bfloat16 [8, 4096, 2048], P('sp', None, 'tp'), may hold values from -0.09375 to 0.09375
- routing: int32 [2048, 2], P('sp'), may hold values from 0 to 7, as said below
- route_weight: float32 [2048, 2], P('sp'), may hold values from 0.1 to 0.9
Outputs:
- layer_out: bfloat16 [2048, 2048], P('sp')
Inputs may be any that keep to these rules, and one draw needn't show every extreme that they name: `routing`: each row names two different experts of one group of 2 consecutive experts. In each aligned block of 256 rows no expert is named by more than 128 rows, and in every block some expert is named by exactly 128 rows.
All inputs are finite; a program needn't handle non-finite values.
Results may differ from a plain program's by a relative error of at most 0.015.
Values may be sent and summed in bfloat16 or wider, within the bound.
A program may use at most 64 MiB of HBM per device.

v0:
```python
import functools
import math

import jax
import jax.numpy as jnp
from jax import lax
from jax.experimental import pallas as pl
from jax.experimental.pallas import tpu as pltpu
from jax.sharding import PartitionSpec as P

GROUPS = 4
SC = jax.named_scope


norm_eps = 1e-06


def online_update(running, query_part, key_part, value_part, query_pos, key_pos, score_scale):
    highest, totals, accum = running
    scores = (
        jnp.einsum("qhd,khd->hqk", query_part, key_part, preferred_element_type=jnp.float32)
        * score_scale
    )
    scores = jnp.where(key_pos[None, None, :] <= query_pos[None, :, None], scores, -jnp.inf)
    new_high = jnp.maximum(highest, jnp.max(scores, axis=-1))
    shrink = jnp.exp(highest - new_high)
    weights = jnp.exp(scores - new_high[:, :, None])
    totals = shrink * totals + jnp.sum(weights, axis=-1)
    blended = jnp.einsum(
        "hqk,khe->qhe", weights.astype(jnp.bfloat16), value_part, preferred_element_type=jnp.float32
    )
    accum = jnp.transpose(shrink)[:, :, None] * accum + blended
    return (new_high, totals, accum)


def shards(
    residual,
    queries,
    key_vectors,
    value_rows,
    head_lambda,
    head_gain,
    out_weight,
    ffn_gain,
    expert_gate,
    expert_up,
    expert_down,
    routing,
    route_weight,
):
    tok_count = queries.shape[0]
    local_heads = queries.shape[1]
    half_width = queries.shape[2] // 2
    value_width = value_rows.shape[2]
    score_scale = half_width ** (-0.5)
    query_pos = lax.axis_index("sp") * tok_count + jnp.arange(tok_count, dtype=jnp.int32)
    last_query = query_pos[-1]
    first_half = queries[:, :, :half_width]
    second_half = queries[:, :, half_width:]
    start_high = jnp.full((local_heads, tok_count), -1e30, jnp.float32)
    start_total = jnp.zeros((local_heads, tok_count), jnp.float32)
    start_accum = jnp.zeros((tok_count, local_heads, value_width), jnp.float32)
    empty_state = (start_high, start_total, start_accum)
    running = (empty_state, empty_state)
    key_piece = lax.all_gather(key_vectors, "sp", axis=0, tiled=True)
    value_piece = lax.all_gather(value_rows, "sp", axis=0, tiled=True)
    piece_len = key_piece.shape[0]
    block_len = math.gcd(piece_len, 512)
    block_count = piece_len // block_len
    key_blocks = key_piece.reshape(block_count, block_len, local_heads, 2 * half_width)
    value_blocks = value_piece.reshape(block_count, block_len, local_heads, value_width)

    def visit(current, stacked):
        block_index, key_block, value_block = stacked
        block_first = block_index * block_len
        key_pos = block_first + jnp.arange(block_len, dtype=jnp.int32)

        def compute(inside):
            first_state = online_update(
                inside[0],
                first_half,
                key_block[:, :, :half_width],
                value_block,
                query_pos,
                key_pos,
                score_scale,
            )
            second_state = online_update(
                inside[1],
                second_half,
                key_block[:, :, half_width:],
                value_block,
                query_pos,
                key_pos,
                score_scale,
            )
            return (first_state, second_state)

        return (lax.cond(block_first <= last_query, compute, lambda inside: inside, current), None)

    running, _ = lax.scan(
        visit, running, (jnp.arange(block_count, dtype=jnp.int32), key_blocks, value_blocks)
    )
    first_state, second_state = running
    first_out = first_state[2] / jnp.transpose(first_state[1])[:, :, None]
    second_out = second_state[2] / jnp.transpose(second_state[1])[:, :, None]
    combined = first_out - head_lambda[None, :, None] * second_out
    normed_heads = (
        combined
        * lax.rsqrt(jnp.mean(combined * combined, axis=-1, keepdims=True) + norm_eps)
        * head_gain
    )
    attended = normed_heads.astype(jnp.bfloat16).reshape(tok_count, local_heads * value_width)
    partial_proj = jnp.dot(attended, out_weight, preferred_element_type=jnp.float32)
    projected = lax.psum(partial_proj.astype(jnp.bfloat16), "tp").astype(jnp.float32)
    stream = residual.astype(jnp.float32) + projected
    block_normed = (
        stream * lax.rsqrt(jnp.mean(stream * stream, axis=-1, keepdims=True) + norm_eps) * ffn_gain
    ).astype(jnp.bfloat16)
    expert_count = lax.axis_size("sp")
    tp_count = lax.axis_size("tp")
    per_group = expert_count // GROUPS
    capacity = tok_count // per_group
    top_count = routing.shape[1]
    model_width = block_normed.shape[1]
    flat_routes = routing.reshape(-1)
    route_count = flat_routes.shape[0]
    onehot = (flat_routes[:, None] == jnp.arange(expert_count, dtype=jnp.int32)[None, :]).astype(
        jnp.int32
    )
    earlier = jnp.cumsum(onehot, axis=0) - onehot
    position = jnp.sum(earlier * onehot, axis=1)
    slot_index = flat_routes * capacity + position
    slot_token = (
        jnp.full((expert_count * capacity,), tok_count, jnp.int32)
        .at[slot_index]
        .set(jnp.arange(route_count, dtype=jnp.int32) // top_count)
    )
    slot_table = slot_token.reshape(expert_count, capacity)
    slice_width = model_width // tp_count
    own_columns = lax.dynamic_slice_in_dim(
        block_normed, lax.axis_index("tp") * slice_width, slice_width, 1
    )
    outgoing = jnp.take(own_columns, slot_table, axis=0, mode="fill", fill_value=0)
    landed = lax.all_to_all(outgoing, "sp", split_axis=0, concat_axis=0, tiled=True)
    arrived = lax.all_gather(landed, "tp", axis=2, tiled=True)
    expert_rows = arrived.reshape(-1, model_width)
    gate_part = jnp.dot(expert_rows, expert_gate[0], preferred_element_type=jnp.float32)
    up_part = jnp.dot(expert_rows, expert_up[0], preferred_element_type=jnp.float32)
    inner_act = (jax.nn.silu(gate_part) * up_part).astype(jnp.bfloat16)
    down_width = expert_down.shape[2]
    weight_rows = expert_down[0]
    expert_sum = jnp.dot(
        lax.all_gather(inner_act, "tp", axis=1, tiled=True),
        weight_rows,
        preferred_element_type=jnp.float32,
    )
    expert_out = expert_sum.astype(jnp.bfloat16).reshape(expert_count, capacity, down_width)
    returned = lax.all_to_all(expert_out, "sp", split_axis=0, concat_axis=0, tiled=True)
    per_route = returned.reshape(expert_count * capacity, down_width)[slot_index]
    weighted = per_route.astype(jnp.float32) * route_weight.reshape(-1)[:, None]
    token_sum = jnp.sum(weighted.reshape(tok_count, top_count, down_width), axis=1)
    moe_rows = lax.all_gather(token_sum.astype(jnp.bfloat16), "tp", axis=1, tiled=True).astype(
        token_sum.dtype
    )
    return (stream + moe_rows).astype(jnp.bfloat16)


MESH = pl.DeviceIdType.MESH
F32 = jnp.float32
BF16 = jnp.bfloat16


def remote(src, dst, send_sem, recv_sem, sp, tp):
    return pltpu.make_async_remote_copy(
        src_ref=src,
        dst_ref=dst,
        send_sem=send_sem,
        recv_sem=recv_sem,
        device_id={"sp": sp, "tp": tp},
        device_id_type=MESH,
    )


def mixed_dot(left, right, contract):
    return lax.dot_general(left, right, (contract, ((), ())), preferred_element_type=F32)


def dispersed(value):
    high = value.astype(BF16)
    rest = value - high.astype(F32)
    middle = rest.astype(BF16)
    low = (rest - middle.astype(F32)).astype(BF16)
    return jnp.concatenate([high, middle, low], axis=0)


def exact_pick(value, picker):
    count = value.shape[0]
    parts = mixed_dot(dispersed(value), picker, ((1,), (0,)))
    return parts[:count] + parts[count : 2 * count] + parts[2 * count :]


def layer_kernel(
    n, tps, cap, heads, head_width,
    q_ref, k_ref, v_ref, route_ref, rw_ref, wd_ref, lam_ref, gain_ref, ow_ref, res_ref, fg_ref,
    gate_ref, up_ref,
    outv,
    raw, resv, owv, sel, selt, stream_ref, normed_ref, meta,
    xs, xall, wg, wu, wdv, hid, keep, away, near, rsend, rrecv, rpass, back, ret,
    kall, vall, rowm, qs, highs, totals, acc, att, part, rbuf, ppass, sq_send, sq_recv,
    in_sem, w_sem, x_send, x_tp, x_sib, x_recv, s_recv, n_send, n_recv, r_send, r_recv,
    b_send, b_recv, o_send, o_recv,
    kv_next, kv_sib, kv_recv, wd_send, wd_recv, m_send, m_recv,
    rs_send, rs_recv, sq_ss, sq_rs, free_sem,
):
    sp = lax.axis_index("sp")
    tp = lax.axis_index("tp")
    z, c = sp // 2, sp % 2
    zs = n // 2
    sib = 2 * z + 1 - c
    toks = resv.shape[0]
    width = heads * head_width
    half = head_width // 2
    piece = normed_ref.shape[1]
    wd_rows = wdv.shape[1]
    experts = n
    per_group = experts // GROUPS
    beside, above, across = tp ^ 1, tp ^ 2, tp ^ 3

    barrier = pltpu.get_barrier_semaphore()
    for d in range(1, n):
        pl.semaphore_signal(
            barrier, inc=1, device_id={"sp": (sp + d) % n, "tp": tp}, device_id_type=MESH
        )
    for d in range(1, tps):
        pl.semaphore_signal(
            barrier, inc=1, device_id={"sp": sp, "tp": (tp + d) % tps}, device_id_type=MESH
        )
    inputs = [
        pltpu.make_async_copy(k_ref, raw.at[0], in_sem.at[0]),
        pltpu.make_async_copy(v_ref, raw.at[1], in_sem.at[1]),
        pltpu.make_async_copy(q_ref, raw.at[2], in_sem.at[2]),
        pltpu.make_async_copy(ow_ref, owv, in_sem.at[3]),
        pltpu.make_async_copy(res_ref, resv, in_sem.at[4]),
    ]
    loads = [
        pltpu.make_async_copy(gate_ref.at[0], wg, w_sem.at[0]),
        pltpu.make_async_copy(up_ref.at[0], wu, w_sem.at[1]),
        pltpu.make_async_copy(
            wd_ref.at[pl.ds(pl.multiple_of(tp * wd_rows, wd_rows), wd_rows), :],
            wdv.at[tp], w_sem.at[2],
        ),
    ]
    for load in inputs + loads:
        load.start()

    run = toks // heads
    spot_row = lax.broadcasted_iota(jnp.int32, (run, toks), 0)
    spot_col = lax.broadcasted_iota(jnp.int32, (run, toks), 1)
    order = jnp.concatenate(
        [(spot_col == spot_row * heads + h).astype(BF16) for h in range(heads)], axis=0
    )

    def split(which, store):
        for i in range(heads):
            rows = jnp.dot(
                order, raw[which, i * toks : (i + 1) * toks, :], preferred_element_type=F32
            )
            for h in range(heads):
                store(i, h, rows[h * run : (h + 1) * run, :])

    def head_rows(h, i=0, count=toks):
        return slice(h * toks + i * run, h * toks + i * run + count)

    def store_keys(i, h, rows):
        kall[sp, head_rows(h, i, run), :] = rows.astype(BF16)

    def store_rows(i, h, rows):
        rowm[head_rows(h, i, run), :] = rows.astype(BF16)

    unit = (
        lax.broadcasted_iota(jnp.int32, (head_width, head_width), 0)
        == lax.broadcasted_iota(jnp.int32, (head_width, head_width), 1)
    ).astype(BF16)

    def turned(h):
        return mixed_dot(unit, rowm[head_rows(h), :], ((1,), (1,)))

    inputs[0].wait()
    split(0, store_keys)
    inputs[1].wait()
    split(1, store_rows)
    for h in range(heads):
        vall[sp, h * head_width : (h + 1) * head_width, :] = turned(h).astype(BF16)

    chunks = 8
    wd_run = wd_rows // chunks

    def wd_copy(k, d):
        to = tp ^ d
        return remote(
            wd_ref.at[pl.ds(pl.multiple_of(to * wd_rows + k * wd_run, wd_run), wd_run), :],
            wdv.at[tp, pl.ds(pl.multiple_of(k * wd_run, wd_run), wd_run)],
            wd_send, wd_recv, sp, to,
        )

    def by_plane(values):
        chosen = values[-1]
        for plane, value in enumerate(values[:-1]):
            chosen = jnp.where(z == plane, value, chosen)
        return chosen

    wd_points = [
        (0, 0, 0, 0), (1, 3, 5, 7), (2, 4, 6, 7), (3, 4, 6, 7), (6, 6, 8, 8), (7, 7, 8, 8), (8, 8, 8, 8)
    ]

    def wd_start(point):
        def start(k, carry):
            for d in (3, 1, 2):
                wd_copy(k, d).start()
            return carry

        lax.fori_loop(by_plane(wd_points[point - 1]), by_plane(wd_points[point]), start, 0)

    class KeyCopies:
        def __init__(self, b, sends, to):
            self.at = (sends.at[b], kv_recv.at[b], to, tp)
            self.block = b

        def start(self):
            for blocks in (kall, vall):
                here = blocks.at[self.block]
                remote(here, here, *self.at).start()

        def wait_send(self):
            both = kall.at[pl.ds(0, 2)]
            remote(both, both, *self.at).wait_send()

        def wait_recv(self):
            both = kall.at[pl.ds(0, 2)]
            remote(both, both, *self.at).wait_recv()

    def next_copy(b):
        return KeyCopies(b, kv_next, sp + 2)

    def kv_sib_copy(b):
        return KeyCopies(b, kv_sib, sib)

    with SC('barrier_wait'):
        pl.semaphore_wait(barrier, n - 1 + tps - 1)

    @pl.when(z < zs - 1)
    def _():
        next_copy(sp).start()

    @pl.when(c == 0)
    def _():
        kv_sib_copy(sp).start()

    wd_start(1)

    depth = lax.broadcasted_iota(jnp.int32, (head_width, toks), 0)
    scale = half ** (-0.5)
    inputs[2].wait()
    split(2, store_rows)
    for h in range(heads):
        columns = turned(h) * scale
        qs[h, :, 0:toks] = jnp.where(depth < half, columns, 0.0).astype(BF16)
        qs[h, :, toks:] = jnp.where(depth >= half, columns, 0.0).astype(BF16)
    highs[...] = jnp.full_like(highs, -1e30)
    totals[...] = jnp.zeros_like(totals)
    acc[...] = jnp.zeros_like(acc)
    rows = lax.broadcasted_iota(jnp.int32, (toks, toks), 0)
    cols = lax.broadcasted_iota(jnp.int32, (toks, toks), 1)
    eye = rows == cols

    def process(b, masked):
        for h in range(heads):
            scores = mixed_dot(kall[b, head_rows(h), :], qs[h], ((1,), (0,)))
            if masked:
                scores = jnp.where(jnp.concatenate([rows <= cols] * 2, axis=1), scores, -1e30)
            old = highs[h]
            high = jnp.maximum(old, jnp.max(scores, axis=0, keepdims=True))
            shrink = jnp.exp(old - high)
            weights = jnp.exp(scores - high)
            totals[h] = shrink * totals[h] + jnp.sum(weights, axis=0, keepdims=True)
            blended = mixed_dot(
                vall[b, h * head_width : (h + 1) * head_width, :], weights.astype(BF16),
                ((1,), (0,)),
            )
            acc[h] = shrink * acc[h] + blended
            highs[h] = high

    with SC('proc_own'):
        process(sp, True)

    first = route_ref[0:1, :]
    lead = lax.broadcasted_iota(jnp.int32, (8, toks), 0)
    member = jnp.logical_and(
        first >= lead * per_group, first < (lead + 1) * per_group
    ).astype(F32)
    earlier = mixed_dot(member.astype(BF16), (rows < cols).astype(BF16), ((1,), (0,)))
    slot = jnp.sum(member * (earlier + lead.astype(F32) * cap), axis=0, keepdims=True)
    slot_col = jnp.sum(jnp.where(eye, slot, 0.0), axis=1, keepdims=True)
    slots = GROUPS * cap
    sel[...] = (
        lax.broadcasted_iota(jnp.int32, (slots, toks), 0) == slot.astype(jnp.int32)
    ).astype(BF16)
    selt[...] = (
        lax.broadcasted_iota(jnp.int32, (toks, slots), 1) == slot_col.astype(jnp.int32)
    ).astype(BF16)
    names = lax.broadcasted_iota(jnp.int32, (experts, toks), 0)
    by_expert = jnp.zeros((experts, toks), F32)
    for k in range(route_ref.shape[0]):
        by_expert = by_expert + jnp.where(
            names == route_ref[k : k + 1, :], rw_ref[k : k + 1, :], 0.0
        )
    by_slot = exact_pick(by_expert, selt[...])
    table = by_slot[:, 0:cap]
    for g in range(1, GROUPS):
        table = table + by_slot[:, g * cap : (g + 1) * cap]
    meta[sp, 0:experts, :] = table

    @pl.when(c == 1)
    def _():
        kv_sib_copy(2 * z).wait_recv()
        process(2 * z, False)

    def give_credits(j):
        def credit(which, plane):
            pl.semaphore_signal(
                free_sem.at[which], inc=1, device_id={"sp": 2 * plane + c, "tp": tp},
                device_id_type=MESH,
            )

        @pl.when(jnp.logical_and(j == z, z == zs - 2))
        def _():
            credit(0, 0)

        @pl.when(jnp.logical_and(j == z, z == zs - 1))
        def _():
            credit(1, 0)
            credit(1, 1)

    def visit(j, carry):
        b = 2 * (z - j) + c
        other = 2 * (z - j) + 1 - c
        with SC('wait_b'):
            kv_sib_copy(b).wait_recv()

        @pl.when(z < zs - 1)
        def _():
            next_copy(b).start()

        kv_sib_copy(b).start()
        give_credits(j)
        with SC('proc_b'):
            process(b, False)
        with SC('wait_o'):
            kv_sib_copy(other).wait_recv()
        with SC('proc_o'):
            process(other, False)
        return carry

    lax.fori_loop(1, z + 1, visit, 0)

    for h in range(heads):
        blend = acc[h] * (1.0 / totals[h])
        mix = blend[:, :toks] - lam_ref[h] * blend[:, toks:]
        mix = mix * lax.rsqrt(jnp.mean(mix * mix, axis=0, keepdims=True) + norm_eps)
        att[:, h * head_width : (h + 1) * head_width] = (mix.T * gain_ref[...]).astype(BF16)
    inputs[3].wait()

    def projected(to):
        return jnp.dot(
            att[...], owv[:, pl.ds(pl.multiple_of(to * piece, piece), piece)],
            preferred_element_type=F32,
        )

    half_toks = toks // 2
    part_halves = (slice(0, half_toks), slice(half_toks, toks))

    def rs_copy(i):
        to, source, target = [
            (beside, part.at[across, part_halves[0]], ppass.at[0]),
            (above, part.at[across, part_halves[1]], ppass.at[1]),
            (beside, part.at[beside, part_halves[0]], rbuf.at[0, part_halves[0]]),
            (above, part.at[above, part_halves[1]], rbuf.at[1, part_halves[1]]),
            (above, part.at[above, part_halves[0]], rbuf.at[1, part_halves[0]]),
            (beside, part.at[beside, part_halves[1]], rbuf.at[0, part_halves[1]]),
        ][i]
        return remote(source, target, rs_send, rs_recv.at[min(i, 2)], sp, to)

    part[across] = projected(across).astype(BF16)
    rs_copy(0).start()
    rs_copy(1).start()
    for_beside = projected(beside)
    part[beside, part_halves[0]] = for_beside[part_halves[0]].astype(BF16)
    rs_copy(2).start()
    for_above = projected(above)
    part[above, part_halves[1]] = for_above[part_halves[1]].astype(BF16)
    rs_copy(3).start()
    mine = pl.ds(pl.multiple_of(tp * piece, piece), piece)
    inputs[4].wait()
    total = resv[:, mine].astype(F32) + projected(tp)
    with SC("rs_pass"):
        rs_copy(0).wait_recv()
    part[above, part_halves[0]] = (for_above[part_halves[0]] + ppass[0].astype(F32)).astype(BF16)
    rs_copy(4).start()
    with SC("rs_pass"):
        rs_copy(1).wait_recv()
    part[beside, part_halves[1]] = (for_beside[part_halves[1]] + ppass[1].astype(F32)).astype(BF16)
    rs_copy(5).start()
    wd_start(2)

    half_cap = cap // 2

    def spot(src, core, part):
        return xall.at[
            src,
            pl.ds(pl.multiple_of(core * cap, cap), cap),
            pl.ds(pl.multiple_of(part * piece, piece), piece),
        ]

    def half_spot(src, part, side):
        return xall.at[
            src,
            pl.ds(pl.multiple_of(c * cap + side * half_cap, half_cap), half_cap),
            pl.ds(pl.multiple_of(part * piece, piece), piece),
        ]

    def x_copy(s):
        group = (z + s) % zs
        return remote(
            xs.at[s], spot(z, c, tp), x_send, x_recv.at[z, 0], 2 * group + c, tp
        )

    def spot_wait(here, sem):
        remote(here, here, x_send, sem, sib, tp).wait_recv()

    def tp_copy(src, i):
        to, side = [(beside, 0), (above, 1), (beside, 1), (above, 0)][i]
        here = half_spot(src, tp, side)
        return remote(here, here, x_tp, x_recv.at[src, 1 + i], sp, to)

    def pass_copy(src, i):
        part, side, to = [(beside, 0, above), (above, 1, beside)][i]
        here = half_spot(src, part, side)
        return remote(here, here, x_tp, x_recv.at[src, 5], sp, to)

    def sib_copy(src, part):
        here = spot(src, c, part)
        return remote(here, here, x_sib, s_recv.at[src], sib, tp)

    def gather(src):
        @pl.when(src != z)
        def _():
            with SC("arrive"):
                spot_wait(spot(src, c, tp), x_recv.at[src, 0])

        for i in range(4):
            tp_copy(src, i).start()
        sib_copy(src, tp).start()

    def gather_pass(src):
        with SC("gpass"):
            spot_wait(half_spot(src, beside, 0), x_recv.at[src, 1])
        pass_copy(src, 0).start()
        with SC("gpass"):
            spot_wait(half_spot(src, above, 1), x_recv.at[src, 2])
        pass_copy(src, 1).start()

    def forward(src):
        with SC("compl_tp"):
            spot_wait(half_spot(src, beside, 1), x_recv.at[src, 3])
            sib_copy(src, beside).start()
            spot_wait(half_spot(src, above, 0), x_recv.at[src, 4])
            sib_copy(src, above).start()
            spot_wait(spot(src, c, across), x_recv.at[src, 5])
            sib_copy(src, across).start()

    def complete(src):
        with SC("compl_sib"):
            spot_wait(
                xall.at[src, pl.ds(pl.multiple_of((1 - c) * cap, cap), cap)], s_recv.at[src]
            )

    pl.when(z > 0)(lambda: gather(0))
    pl.when(z == zs - 2)(lambda: gather(1))

    with SC("rs_wait"):
        remote(rbuf, rbuf, rs_send, rs_recv.at[2], sp, beside).wait_recv()
    total = total + rbuf[0].astype(F32) + rbuf[1].astype(F32)
    stream_ref[...] = total
    normed_ref[...] = (total * fg_ref[:, mine]).astype(BF16)
    squares = jnp.sum(total * total, axis=1, keepdims=True)
    as_row = jnp.sum(jnp.where(eye, squares, 0.0), axis=0, keepdims=True)
    sq_send[...] = jnp.broadcast_to(as_row, sq_send.shape)

    def sq_copy(d):
        return remote(
            sq_send, sq_recv.at[d], sq_ss, sq_rs, sp, (tp + d) % tps
        )

    for d in range(1, tps):
        sq_copy(d).start()

    def m_copy(d):
        return remote(meta.at[sp], meta.at[sp], m_send, m_recv.at[sp], (sp + d) % n, tp)

    def m_wait(src):
        @pl.when(src != sp)
        def _():
            remote(meta.at[src], meta.at[src], m_send, m_recv.at[src], sib, tp).wait_recv()

    for s in list(range(1, zs)) + [0]:
        group = (z + s) % zs
        picked = jnp.dot(
            sel[pl.ds(pl.multiple_of(group * cap, cap), cap), :], normed_ref[...],
            preferred_element_type=F32,
        ).astype(BF16)
        if s:
            xs[s] = picked
            pl.when(z >= (zs - s if s >= zs - 2 else 0))(lambda: x_copy(s).start())
        else:
            spot(z, c, tp)[...] = picked

    @pl.when(z < zs - 1)
    def _():
        gather(z)

    wd_start(3)

    def row_factors():
        with SC("sq_wait"):
            squares_in = sq_recv.at[pl.ds(1, tps - 1)]
            remote(squares_in, squares_in, sq_ss, sq_rs, sp, beside).wait_recv()
        sums = sq_send[0:1, :]
        for d in range(1, tps):
            sums = sums + sq_recv[d, 0:1, :]
        inverse = lax.rsqrt(sums * (1.0 / (piece * tps)) + norm_eps)
        by_slot = exact_pick(jnp.broadcast_to(inverse, (8, toks)), selt[...])
        for g in range(GROUPS):
            meta[sp, experts + g : experts + g + 1, :] = by_slot[0:1, g * cap : (g + 1) * cap]
        for d in range(1, n):
            m_copy(d).start()

    def late_rows(s, which):
        with SC("credit"):
            pl.semaphore_wait(free_sem.at[which], 1)
        x_copy(s).start()

    pl.when(z < zs - 2)(row_factors)
    gather_pass(0)

    @pl.when(z == zs - 2)
    def _():
        gather_pass(1)
        gather_pass(2)

    pl.when(z == zs - 1)(lambda: gather(1))
    wd_start(4)
    pl.when(z == zs - 2)(row_factors)
    pl.when(z == 1)(lambda: late_rows(zs - 2, 1))

    @pl.when(z == 0)
    def _():
        late_rows(zs - 2, 0)
        gather(1)
        late_rows(zs - 1, 1)

    def late_sources():
        gather(zs - 2)
        pl.when(z == 0)(lambda: gather_pass(1))
        wd_start(5)
        forward(1)
        gather_pass(zs - 2)
        wd_start(6)

    def near_copy(src, part):
        return remote(
            away.at[src, part], near.at[src, part], n_send,
            n_recv.at[src, jnp.where(part == across, 0, 1)], sib, tp,
        )

    def near_wait(src, first):
        here = near.at[src, pl.ds(0, 1 if first else tps - 1)]
        remote(here, here, n_send, n_recv.at[src, 0 if first else 1], sib, tp).wait_recv()

    tile = 256
    small_eye = lax.broadcasted_iota(jnp.int32, (cap, cap), 0) == lax.broadcasted_iota(
        jnp.int32, (cap, cap), 1
    )
    which = lax.broadcasted_iota(jnp.int32, meta.shape[1:], 0)

    def meta_col(src, core, line):
        row = jnp.sum(jnp.where(which == line, meta[2 * src + core], 0.0), axis=0, keepdims=True)
        return jnp.sum(jnp.where(small_eye, row, 0.0), axis=1, keepdims=True)

    keep_rows = pl.ds(pl.multiple_of(c * cap, cap), cap)
    away_rows = pl.ds(pl.multiple_of((1 - c) * cap, cap), cap)

    def ffn_one(src, between):
        @pl.when(src == 0)
        def _():
            for load in loads:
                load.wait()

        with SC("m_wait"):
            m_wait(2 * src)
            m_wait(2 * src + 1)
        factor = jnp.concatenate(
            [meta_col(src, c, experts + z), meta_col(src, 1 - c, experts + z)], axis=0
        )

        def one(i, carry):
            pl.when(i == wg.shape[1] // tile // 2)(between)
            at = pl.ds(pl.multiple_of(i * tile, tile), tile)
            x = jnp.concatenate([xall[src, keep_rows], xall[src, away_rows]], axis=0)
            gate = jnp.dot(x, wg[:, at], preferred_element_type=F32) * factor
            up = jnp.dot(x, wu[:, at], preferred_element_type=F32) * factor
            hid[src, :, at] = (gate / (1.0 + jnp.exp(-gate)) * up).astype(BF16)
            return carry

        with SC("ffn_one"):
            lax.fori_loop(0, wg.shape[1] // tile, one, 0)

    def ffn_two(src):
        @pl.when(src == 0)
        def _():
            with SC("down_wait"):
                others = wdv.at[pl.ds(0, tps - 1)]
                remote(others, others, wd_send, wd_recv, sp, beside).wait()

        row_weight = jnp.concatenate(
            [meta_col(src, c, sp), meta_col(src, 1 - c, sp)], axis=0
        )

        def two(j, carry):
            to = tp ^ (tps - 1 - j)
            result = jnp.dot(hid[src], wdv[to], preferred_element_type=F32) * row_weight
            away[src, to] = result[cap:].astype(BF16)
            near_copy(src, to).start()
            keep[src, to] = result[:cap]
            return carry

        with SC("ffn_two"):
            lax.fori_loop(0, tps, two, 0)

    cap_halves = (slice(0, half_cap), slice(half_cap, cap))

    def r_copy(src, i):
        to, source, target = [
            (beside, rsend.at[src, across, cap_halves[0]], rpass.at[src, 0]),
            (above, rsend.at[src, across, cap_halves[1]], rpass.at[src, 1]),
            (beside, rsend.at[src, beside, cap_halves[0]], rrecv.at[src, 0, cap_halves[0]]),
            (above, rsend.at[src, above, cap_halves[1]], rrecv.at[src, 1, cap_halves[1]]),
            (above, rsend.at[src, above, cap_halves[0]], rrecv.at[src, 1, cap_halves[0]]),
            (beside, rsend.at[src, beside, cap_halves[1]], rrecv.at[src, 0, cap_halves[1]]),
        ][i]
        return remote(source, target, r_send, r_recv.at[src, min(i, 2)], sp, to)

    def both(src, to, at):
        return keep[src, to, at, :] + near[src, to, at, :].astype(F32)

    def spread(src):
        with SC("near_wait"):
            near_wait(src, True)
        rsend[src, across] = both(src, across, slice(0, cap)).astype(BF16)
        r_copy(src, 0).start()
        r_copy(src, 1).start()
        near_wait(src, False)
        rsend[src, above, cap_halves[1]] = both(src, above, cap_halves[1]).astype(BF16)
        r_copy(src, 3).start()
        rsend[src, beside, cap_halves[0]] = both(src, beside, cap_halves[0]).astype(BF16)
        r_copy(src, 2).start()

    def spread_pass(src):
        with SC("spass"):
            r_copy(src, 0).wait_recv()
        rsend[src, above, cap_halves[0]] = (
            both(src, above, cap_halves[0]) + rpass[src, 0].astype(F32)
        ).astype(BF16)
        r_copy(src, 4).start()
        with SC("spass"):
            r_copy(src, 1).wait_recv()
        rsend[src, beside, cap_halves[1]] = (
            both(src, beside, cap_halves[1]) + rpass[src, 1].astype(F32)
        ).astype(BF16)
        r_copy(src, 5).start()

    def b_copy(src):
        return remote(
            back.at[src], ret.at[z], b_send, b_recv, 2 * src + c, tp
        )

    def finish(src):
        with SC("r_wait"):
            here = rrecv.at[src]
            remote(here, here, r_send, r_recv.at[src, 2], sp, beside).wait_recv()
        total = both(src, tp, slice(0, cap))
        total = total + rrecv[src, 0].astype(F32) + rrecv[src, 1].astype(F32)

        @pl.when(src == z)
        def _():
            ret[z] = total.astype(BF16)

        @pl.when(src != z)
        def _():
            back[src] = total.astype(BF16)
            b_copy(src).start()

    last = zs - 1

    at_last = z == last

    early = z < last

    def when_both(one, two):
        return pl.when(jnp.logical_and(one, two))

    third = z == last - 1
    first_two = z < last - 1

    def up_step(s):
        def between():
            when_both(third, s == 0)(lambda: forward(1))
            when_both(z == 1, s == 0)(lambda: gather_pass(1))
            when_both(early, s == 1)(lambda: forward(2))
            when_both(early, s == last - 1)(lambda: gather(last))
            when_both(third, s == last)(lambda: spread_pass(1))
            when_both(at_last, s < last)(lambda: gather_pass(s + 1))
            when_both(at_last, s + 2 <= last)(lambda: gather(s + 2))

        pl.when(s == 0)(lambda: forward(0))
        when_both(first_two, s == 1)(late_sources)
        complete(s)
        ffn_one(s, between)
        when_both(z != last - 1, s == last)(lambda: spread_pass(last - 1))
        when_both(early, s == last)(lambda: finish(0))
        when_both(first_two, s == last)(lambda: finish(1))

    def down_step(s):
        ffn_two(s)
        when_both(at_last, s < last)(lambda: forward(s + 1))
        when_both(s >= 1, jnp.where(third, s == 1, s < last))(lambda: spread_pass(s - 1))
        when_both(third, s == last - 1)(lambda: spread_pass(last))
        spread(s)
        when_both(early, s == 0)(lambda: gather_pass(last))
        pl.when(jnp.where(third, s == 1, jnp.logical_and(first_two, s == last - 1)))(
            lambda: forward(last)
        )
        when_both(at_last, s == 0)(row_factors)
        when_both(at_last, s == last - 1)(lambda: finish(0))
        when_both(z >= last - 1, s == last)(lambda: finish(1))
        when_both(z != last - 1, s == last)(lambda: finish(2))

    def step(k, carry):
        turn = k
        for at, (one, two) in enumerate(
            ((0, 0), (2, 2), (4, 4), (1, 1), (3, 3), (5, 6), (6, 7), (7, 5))
        ):
            turn = jnp.where(jnp.logical_and(first_two, k == at), one, turn)
            turn = jnp.where(jnp.logical_and(third, k == at), two, turn)
        pl.when(turn % 2 == 0)(lambda: up_step(turn // 2))
        pl.when(turn % 2 == 1)(lambda: down_step(turn // 2))
        return carry

    lax.fori_loop(0, 2 * zs, step, 0)
    pl.when(z != last - 1)(lambda: spread_pass(last))
    pl.when(third)(lambda: spread_pass(last - 1))
    finish(last)
    pl.when(third)(lambda: finish(last - 1))

    with SC("b_wait"):
        returns = ret.at[pl.ds(0, zs - 1)]
        remote(returns, returns, b_send, b_recv, sib, tp).wait_recv()
    rows = ret[...].reshape(zs * cap, piece)
    layer = stream_ref[...] + jnp.dot(selt[...], rows, preferred_element_type=F32)
    outv[:, mine] = layer.astype(BF16)

    def out_spot(part, side):
        return outv.at[part_halves[side], pl.ds(pl.multiple_of(part * piece, piece), piece)]

    def o_copy(i):
        part, side, to = [
            (tp, 0, beside), (tp, 1, above), (tp, 1, beside), (tp, 0, above),
            (beside, 0, above), (above, 1, beside),
        ][i]
        here = out_spot(part, side)
        return remote(here, here, o_send, o_recv.at[min(i, 4)], sp, to)

    def o_wait(part, i, side=None):
        at = pl.ds(pl.multiple_of(part * piece, piece), piece)
        here = outv.at[:, at] if side is None else out_spot(part, side)
        remote(here, here, o_send, o_recv.at[i], sib, tp).wait_recv()

    for i in range(4):
        o_copy(i).start()
    with SC("o_pass"):
        o_wait(beside, 0, 0)
    o_copy(4).start()
    with SC("o_pass"):
        o_wait(above, 1, 1)
    o_copy(5).start()

    def sent(here, sem):
        remote(here, here, sem, kv_recv.at[0], sib, tp).wait_send()

    sent(sq_recv.at[pl.ds(1, tps - 1)], sq_ss)
    sent(part.at[pl.ds(0, 3)], rs_send)
    sent(meta.at[pl.ds(0, n - 1)], m_send)
    sent(xs.at[pl.ds(1, zs - 1)], x_send)
    sent(back.at[pl.ds(0, zs - 1)], b_send)
    sent(away, n_send)
    sent(away, x_sib)
    sent(away.at[pl.ds(0, zs - 1)], x_tp)
    sent(away.at[pl.ds(0, zs - 1)], r_send)

    @pl.when(z < zs - 1)
    def _():
        next_copy(sp).wait_send()

    @pl.when(c == 0)
    def _():
        kv_sib_copy(sp).wait_send()

    def drain(j, carry):
        b = 2 * (z - j) + c

        @pl.when(z < zs - 1)
        def _():
            next_copy(b).wait_send()

        kv_sib_copy(b).wait_send()
        return carry

    lax.fori_loop(1, z + 1, drain, 0)
    with SC("o_wait"):
        o_wait(beside, 2, 1)
        o_wait(above, 3, 0)
        o_wait(across, 4)
    with SC("o_send"):
        sent(part.at[pl.ds(0, 3)], o_send)


def paired_shards(
    residual, queries, key_vectors, value_rows, head_lambda, head_gain, out_weight, ffn_gain,
    expert_gate, expert_up, expert_down, routing, route_weight,
):
    n = lax.axis_size("sp")
    tps = lax.axis_size("tp")
    toks, heads, head_width = queries.shape
    width = heads * head_width
    model = residual.shape[1]
    piece = model // tps
    experts = n
    per_group = experts // GROUPS
    cap = toks // per_group
    down = expert_down[0]
    wd_rows = down.shape[0] // tps
    vmem = pl.BlockSpec(memory_space=pltpu.VMEM)
    smem = pl.BlockSpec(memory_space=pltpu.SMEM)
    hbm = pl.BlockSpec(memory_space=pltpu.HBM)
    dma = pltpu.SemaphoreType.DMA
    zs = n // 2
    def stay(x):
        return pltpu.with_memory_space_constraint(x, pltpu.HBM)

    return pl.pallas_call(
        functools.partial(layer_kernel, n, tps, cap, heads, head_width),
        out_shape=jax.ShapeDtypeStruct((toks, model), BF16),
        in_specs=[hbm, hbm, hbm, vmem, vmem, hbm, smem, vmem, hbm, hbm, vmem, hbm, hbm],
        out_specs=vmem,
        scratch_shapes=[
            pltpu.VMEM((3, toks * heads, head_width), BF16),
            pltpu.VMEM((toks, model), BF16),
            pltpu.VMEM((width, model), BF16),
            pltpu.VMEM((GROUPS * cap, toks), BF16),
            pltpu.VMEM((toks, GROUPS * cap), BF16),
            pltpu.VMEM((toks, piece), F32),
            pltpu.VMEM((toks, piece), BF16),
            pltpu.VMEM((n, experts + 8, cap), F32),
            pltpu.VMEM((zs, cap, piece), BF16),
            pltpu.VMEM((zs, 2 * cap, model), BF16),
            pltpu.VMEM(expert_gate.shape[1:], BF16),
            pltpu.VMEM(expert_up.shape[1:], BF16),
            pltpu.VMEM((tps, wd_rows, piece), BF16),
            pltpu.VMEM((zs, 2 * cap, expert_gate.shape[2]), BF16),
            pltpu.VMEM((zs, tps, cap, piece), F32),
            pltpu.VMEM((zs, tps, cap, piece), BF16),
            pltpu.VMEM((zs, tps, cap, piece), BF16),
            pltpu.VMEM((zs, tps, cap, piece), BF16),
            pltpu.VMEM((zs, 2, cap, piece), BF16),
            pltpu.VMEM((zs, 2, cap // 2, piece), BF16),
            pltpu.VMEM((zs, cap, piece), BF16),
            pltpu.VMEM((zs, cap, piece), BF16),
            pltpu.VMEM((n, heads * toks, head_width), BF16),
            pltpu.VMEM((n, width, toks), BF16),
            pltpu.VMEM((heads * toks, head_width), BF16),
            pltpu.VMEM((heads, head_width, 2 * toks), BF16),
            pltpu.VMEM((heads, 1, 2 * toks), F32),
            pltpu.VMEM((heads, 1, 2 * toks), F32),
            pltpu.VMEM((heads, head_width, 2 * toks), F32),
            pltpu.VMEM((toks, width), BF16),
            pltpu.VMEM((tps, toks, piece), BF16),
            pltpu.VMEM((2, toks, piece), BF16),
            pltpu.VMEM((2, toks // 2, piece), BF16),
            pltpu.VMEM((8, toks), F32),
            pltpu.VMEM((tps, 8, toks), F32),
            dma((5,)), dma((3,)),
            dma, dma, dma, dma((zs, 6)), dma((zs,)),
            dma, dma((zs, 2)), dma, dma((zs, 3)),
            dma, dma, dma, dma((5,)),
            dma((n,)), dma((n,)), dma((n,)),
            dma, dma, dma, dma((n,)),
            dma, dma((3,)), dma, dma, pltpu.SemaphoreType.REGULAR((2,)),
        ],
        compiler_params=pltpu.CompilerParams(collective_id=0, has_side_effects=True, vmem_limit_bytes=49545216),
        name="layer",
    )(
        stay(queries.reshape(toks * heads, head_width)), stay(key_vectors.reshape(toks * heads, head_width)),
        stay(value_rows.reshape(toks * heads, head_width)), stay(routing.T), stay(route_weight.T), stay(down),
        stay(head_lambda), stay(head_gain.reshape(1, -1)), stay(out_weight), stay(residual), stay(ffn_gain.reshape(1, -1)),
        stay(expert_gate), stay(expert_up),
    )


def solution(mesh):
    in_specs = (
        P("sp", None),
        P("sp", "tp", None),
        P("sp", "tp", None),
        P("sp", "tp", None),
        P("tp"),
        P(),
        P("tp", None),
        P(),
        P("sp", None, "tp"),
        P("sp", None, "tp"),
        P("sp", None, "tp"),
        P("sp", None),
        P("sp", None),
    )
    out_specs = P("sp", None)
    paired = mesh.shape["sp"] == 2 * GROUPS and mesh.shape["tp"] == 4
    return jax.shard_map(paired_shards if paired else shards, mesh=mesh, in_specs=in_specs, out_specs=out_specs, check_vma=False)
```

profile of v0, /device:TPU:24, one launch (start us, length us, event | category | flops | bytes accessed | tf_op | source)
XLA Modules:
  0.0 120.6 jit_solution(14138735830090638732)
XLA Ops:
  0.0 119.6 %layer.1 = bf16[256,2048]{1,0:T(8,128)(2,1)S(1)} custom-call(bf16[1024,128]{1,0:T(8,128)(2,1)} %bitcast.9, bf16[1024,128]{1,0:T(8,128)(2,1)} %bitcast.10, bf16[1024,128]{1,0:T(8,128)(2,1)} %bitcast.11, s32[2,256]{1,0:T(2,128)} %bitcast.13, f32[2,256]{1,0:T(2,128)} %bitcast.14, bf16[4096,512]{1,0:T(8,128)(2,1)} %bitcast.8, f32[4]{0:T(128)} %lam_ref.1, ...), custom_call_target="tpu_custom_call" | custom-call | tf_op jit(solution)/shard_map/layer/pallas_call | solution.py:970
  119.6 1.0 copy.15
where the time goes:
time: 121 us
  Pallas kernels  120 us (99%)
    pallas_call x1, Pallas kernels, paired_shards(): pl.pallas_call(functools.partial(layer_kernel, n, tps, cap, heads, head_w...  120 us

commit v1 on v0

--- a/solution.py
+++ b/solution.py
@@ -202,10 +202,10 @@
 
 def layer_kernel(
     n, tps, cap, heads, head_width,
-    q_ref, k_ref, v_ref, route_ref, rw_ref, wd_ref, lam_ref, gain_ref, ow_ref, res_ref, fg_ref,
+    q_ref, k_ref, v_ref, route_in, rw_in, wd_ref, lam_in, gain_in, ow_ref, res_ref, fg_in,
     gate_ref, up_ref,
     outv,
-    raw, resv, owv, sel, selt, stream_ref, normed_ref, meta,
+    route_ref, rw_ref, lam_ref, gain_ref, fg_ref, raw, resv, owv, sel, selt, stream_ref, normed_ref, meta,
     xs, xall, wg, wu, wdv, hid, keep, away, near, rsend, rrecv, rpass, back, ret,
     kall, vall, rowm, qs, highs, totals, acc, att, part, rbuf, ppass, sq_send, sq_recv,
     in_sem, w_sem, x_send, x_tp, x_sib, x_recv, s_recv, n_send, n_recv, r_send, r_recv,
@@ -243,6 +243,15 @@
         pltpu.make_async_copy(ow_ref, owv, in_sem.at[3]),
         pltpu.make_async_copy(res_ref, resv, in_sem.at[4]),
     ]
+    small = [
+        pltpu.make_async_copy(given, kept, in_sem.at[5 + i])
+        for i, (given, kept) in enumerate(
+            (
+                (route_in, route_ref), (rw_in, rw_ref), (lam_in, lam_ref), (gain_in, gain_ref),
+                (fg_in, fg_ref),
+            )
+        )
+    ]
     loads = [
         pltpu.make_async_copy(gate_ref.at[0], wg, w_sem.at[0]),
         pltpu.make_async_copy(up_ref.at[0], wu, w_sem.at[1]),
@@ -251,7 +260,7 @@
             wdv.at[tp], w_sem.at[2],
         ),
     ]
-    for load in inputs + loads:
+    for load in inputs + small + loads:
         load.start()
 
     run = toks // heads
@@ -394,6 +403,8 @@
     with SC('proc_own'):
         process(sp, True)
 
+    for load in small:
+        load.wait()
     first = route_ref[0:1, :]
     lead = lax.broadcasted_iota(jnp.int32, (8, toks), 0)
     member = jnp.logical_and(
@@ -466,7 +477,7 @@
 
     for h in range(heads):
         blend = acc[h] * (1.0 / totals[h])
-        mix = blend[:, :toks] - lam_ref[h] * blend[:, toks:]
+        mix = blend[:, :toks] - lam_ref[:, h : h + 1] * blend[:, toks:]
         mix = mix * lax.rsqrt(jnp.mean(mix * mix, axis=0, keepdims=True) + norm_eps)
         att[:, h * head_width : (h + 1) * head_width] = (mix.T * gain_ref[...]).astype(BF16)
     inputs[3].wait()
@@ -725,8 +736,8 @@
         with SC("ffn_one"):
             lax.fori_loop(0, wg.shape[1] // tile, one, 0)
 
-    def ffn_two(src):
-        @pl.when(src == 0)
+    def ffn_two(src, first):
+        @pl.when(first)
         def _():
             with SC("down_wait"):
                 others = wdv.at[pl.ds(0, tps - 1)]
@@ -821,6 +832,8 @@
 
     third = z == last - 1
     first_two = z < last - 1
+    lead = jnp.where(first_two, last - 1, 0)
+    after = jnp.where(z == 1, 0, 1)
 
     def up_step(s):
         def between():
@@ -828,49 +841,53 @@
             when_both(z == 1, s == 0)(lambda: gather_pass(1))
             when_both(early, s == 1)(lambda: forward(2))
             when_both(early, s == last - 1)(lambda: gather(last))
-            when_both(third, s == last)(lambda: spread_pass(1))
+            when_both(early, s == last)(lambda: finish(lead))
+            when_both(early, s == last)(lambda: spread_pass(after))
             when_both(at_last, s < last)(lambda: gather_pass(s + 1))
             when_both(at_last, s + 2 <= last)(lambda: gather(s + 2))
 
         pl.when(s == 0)(lambda: forward(0))
+        when_both(at_last, s == 0)(row_factors)
         when_both(first_two, s == 1)(late_sources)
         complete(s)
         ffn_one(s, between)
-        when_both(z != last - 1, s == last)(lambda: spread_pass(last - 1))
-        when_both(early, s == last)(lambda: finish(0))
-        when_both(first_two, s == last)(lambda: finish(1))
+        when_both(at_last, s == last)(lambda: spread_pass(last - 1))
 
     def down_step(s):
-        ffn_two(s)
+        ffn_two(s, s == jnp.where(early, lead, 0))
         when_both(at_last, s < last)(lambda: forward(s + 1))
-        when_both(s >= 1, jnp.where(third, s == 1, s < last))(lambda: spread_pass(s - 1))
-        when_both(third, s == last - 1)(lambda: spread_pass(last))
+        when_both(early, s == lead)(lambda: gather_pass(last))
+        when_both(early, s == after)(lambda: spread_pass(lead))
+        when_both(early, s == z)(lambda: spread_pass(last))
+        when_both(at_last, jnp.logical_and(s >= 1, s < last))(lambda: spread_pass(s - 1))
         spread(s)
-        when_both(early, s == 0)(lambda: gather_pass(last))
-        pl.when(jnp.where(third, s == 1, jnp.logical_and(first_two, s == last - 1)))(
-            lambda: forward(last)
-        )
-        when_both(at_last, s == 0)(row_factors)
+        when_both(early, s == after)(lambda: forward(last))
+        when_both(early, s == last)(lambda: finish(after))
         when_both(at_last, s == last - 1)(lambda: finish(0))
-        when_both(z >= last - 1, s == last)(lambda: finish(1))
-        when_both(z != last - 1, s == last)(lambda: finish(2))
+
+        @pl.when(jnp.logical_and(at_last, s == last))
+        def _():
+            finish(1)
+            finish(2)
 
     def step(k, carry):
         turn = k
-        for at, (one, two) in enumerate(
-            ((0, 0), (2, 2), (4, 4), (1, 1), (3, 3), (5, 6), (6, 7), (7, 5))
+        for at, value in enumerate(
+            (0, 2, 4, 2 * lead + 1, 2 * after + 1, 2 * last, 2 * last + 1, 2 * z + 1)
         ):
-            turn = jnp.where(jnp.logical_and(first_two, k == at), one, turn)
-            turn = jnp.where(jnp.logical_and(third, k == at), two, turn)
+            turn = jnp.where(jnp.logical_and(early, k == at), value, turn)
         pl.when(turn % 2 == 0)(lambda: up_step(turn // 2))
         pl.when(turn % 2 == 1)(lambda: down_step(turn // 2))
         return carry
 
     lax.fori_loop(0, 2 * zs, step, 0)
-    pl.when(z != last - 1)(lambda: spread_pass(last))
-    pl.when(third)(lambda: spread_pass(last - 1))
+    pl.when(at_last)(lambda: spread_pass(last))
     finish(last)
-    pl.when(third)(lambda: finish(last - 1))
+
+    @pl.when(early)
+    def _():
+        spread_pass(z)
+        finish(z)
 
     with SC("b_wait"):
         returns = ret.at[pl.ds(0, zs - 1)]
@@ -960,7 +977,6 @@
     down = expert_down[0]
     wd_rows = down.shape[0] // tps
     vmem = pl.BlockSpec(memory_space=pltpu.VMEM)
-    smem = pl.BlockSpec(memory_space=pltpu.SMEM)
     hbm = pl.BlockSpec(memory_space=pltpu.HBM)
     dma = pltpu.SemaphoreType.DMA
     zs = n // 2
@@ -970,9 +986,14 @@
     return pl.pallas_call(
         functools.partial(layer_kernel, n, tps, cap, heads, head_width),
         out_shape=jax.ShapeDtypeStruct((toks, model), BF16),
-        in_specs=[hbm, hbm, hbm, vmem, vmem, hbm, smem, vmem, hbm, hbm, vmem, hbm, hbm],
+        in_specs=[hbm] * 13,
         out_specs=vmem,
         scratch_shapes=[
+            pltpu.VMEM(routing.shape[::-1], jnp.int32),
+            pltpu.VMEM(route_weight.shape[::-1], F32),
+            pltpu.VMEM((1, heads), F32),
+            pltpu.VMEM((1, head_width), F32),
+            pltpu.VMEM((1, model), F32),
             pltpu.VMEM((3, toks * heads, head_width), BF16),
             pltpu.VMEM((toks, model), BF16),
             pltpu.VMEM((width, model), BF16),
@@ -1008,7 +1029,7 @@
             pltpu.VMEM((2, toks // 2, piece), BF16),
             pltpu.VMEM((8, toks), F32),
             pltpu.VMEM((tps, 8, toks), F32),
-            dma((5,)), dma((3,)),
+            dma((10,)), dma((3,)),
             dma, dma, dma, dma((zs, 6)), dma((zs,)),
             dma, dma((zs, 2)), dma, dma((zs, 3)),
             dma, dma, dma, dma((5,)),
@@ -1021,7 +1042,7 @@
     )(
         stay(queries.reshape(toks * heads, head_width)), stay(key_vectors.reshape(toks * heads, head_width)),
         stay(value_rows.reshape(toks * heads, head_width)), stay(routing.T), stay(route_weight.T), stay(down),
-        stay(head_lambda), stay(head_gain.reshape(1, -1)), stay(out_weight), stay(residual), stay(ffn_gain.reshape(1, -1)),
+        stay(head_lambda.reshape(1, -1)), stay(head_gain.reshape(1, -1)), stay(out_weight), stay(residual), stay(ffn_gain.reshape(1, -1)),
         stay(expert_gate), stay(expert_up),
     )
 

time: 121 us -> 118 us (0.975)
  Pallas kernels: 120 us -> 117 us
    pallas_call x1, Pallas kernels: 120 us -> 117 us  [paired_shards(): pl.pallas_call(functools.partial(layer_kernel, n, tps, cap, heads, head_w...]
where the time goes in v1:
time: 118 us
  Pallas kernels  117 us (99%)
    pallas_call x1, Pallas kernels, paired_shards(): pl.pallas_call(functools.partial(layer_kernel, n, tps, cap, heads, head_w...  117 us

profile of v1, /device:TPU:24, one launch (start us, length us, event | category | flops | bytes accessed | tf_op | source)
XLA Modules:
  0.0 118.2 jit_solution(2262187522936111161)
XLA Ops:
  0.0 117.3 %layer.1 = bf16[256,2048]{1,0:T(8,128)(2,1)S(1)} custom-call(bf16[1024,128]{1,0:T(8,128)(2,1)} %bitcast.10, bf16[1024,128]{1,0:T(8,128)(2,1)} %bitcast.11, bf16[1024,128]{1,0:T(8,128)(2,1)} %bitcast.12, s32[2,256]{1,0:T(2,128)} %bitcast.14, f32[2,256]{1,0:T(2,128)} %bitcast.15, bf16[4096,512]{1,0:T(8,128)(2,1)} %bitcast.9, f32[1,4]{1,0:T(1,128)} %bitcast.16, ...), custom_call_target="tpu_custom_call" | custom-call | tf_op jit(solution)/shard_map/layer/pallas_call | solution.py:986
  117.3 1.0 copy.15

commit v2 on v1

--- a/solution.py
+++ b/solution.py
@@ -333,7 +333,7 @@
 
     class KeyCopies:
         def __init__(self, b, sends, to):
-            self.at = (sends.at[b], kv_recv.at[b], to, tp)
+            self.at = (sends.at[b // 2], kv_recv.at[b], to, tp)
             self.block = b
 
         def start(self):
@@ -552,12 +552,12 @@
     def tp_copy(src, i):
         to, side = [(beside, 0), (above, 1), (beside, 1), (above, 0)][i]
         here = half_spot(src, tp, side)
-        return remote(here, here, x_tp, x_recv.at[src, 1 + i], sp, to)
+        return remote(here, here, x_tp, x_recv.at[src, 1 + i // 2], sp, to)
 
     def pass_copy(src, i):
         part, side, to = [(beside, 0, above), (above, 1, beside)][i]
         here = half_spot(src, part, side)
-        return remote(here, here, x_tp, x_recv.at[src, 5], sp, to)
+        return remote(here, here, x_tp, x_recv.at[src, 3], sp, to)
 
     def sib_copy(src, part):
         here = spot(src, c, part)
@@ -575,19 +575,16 @@
 
     def gather_pass(src):
         with SC("gpass"):
-            spot_wait(half_spot(src, beside, 0), x_recv.at[src, 1])
+            spot_wait(spot(src, c, beside), x_recv.at[src, 1])
         pass_copy(src, 0).start()
-        with SC("gpass"):
-            spot_wait(half_spot(src, above, 1), x_recv.at[src, 2])
         pass_copy(src, 1).start()
 
     def forward(src):
         with SC("compl_tp"):
-            spot_wait(half_spot(src, beside, 1), x_recv.at[src, 3])
+            spot_wait(spot(src, c, beside), x_recv.at[src, 2])
             sib_copy(src, beside).start()
-            spot_wait(half_spot(src, above, 0), x_recv.at[src, 4])
             sib_copy(src, above).start()
-            spot_wait(spot(src, c, across), x_recv.at[src, 5])
+            spot_wait(spot(src, c, across), x_recv.at[src, 3])
             sib_copy(src, across).start()
 
     def complete(src):
@@ -698,7 +695,7 @@
         here = near.at[src, pl.ds(0, 1 if first else tps - 1)]
         remote(here, here, n_send, n_recv.at[src, 0 if first else 1], sib, tp).wait_recv()
 
-    tile = 256
+    tile = 512
     small_eye = lax.broadcasted_iota(jnp.int32, (cap, cap), 0) == lax.broadcasted_iota(
         jnp.int32, (cap, cap), 1
     )
@@ -769,7 +766,7 @@
             (above, rsend.at[src, above, cap_halves[0]], rrecv.at[src, 1, cap_halves[0]]),
             (beside, rsend.at[src, beside, cap_halves[1]], rrecv.at[src, 0, cap_halves[1]]),
         ][i]
-        return remote(source, target, r_send, r_recv.at[src, min(i, 2)], sp, to)
+        return remote(source, target, r_send, r_recv.at[src, min(i // 2, 1)], sp, to)
 
     def both(src, to, at):
         return keep[src, to, at, :] + near[src, to, at, :].astype(F32)
@@ -788,13 +785,12 @@
 
     def spread_pass(src):
         with SC("spass"):
-            r_copy(src, 0).wait_recv()
+            passed = rpass.at[src]
+            remote(passed, passed, r_send, r_recv.at[src, 0], sp, beside).wait_recv()
         rsend[src, above, cap_halves[0]] = (
             both(src, above, cap_halves[0]) + rpass[src, 0].astype(F32)
         ).astype(BF16)
         r_copy(src, 4).start()
-        with SC("spass"):
-            r_copy(src, 1).wait_recv()
         rsend[src, beside, cap_halves[1]] = (
             both(src, beside, cap_halves[1]) + rpass[src, 1].astype(F32)
         ).astype(BF16)
@@ -808,7 +804,7 @@
     def finish(src):
         with SC("r_wait"):
             here = rrecv.at[src]
-            remote(here, here, r_send, r_recv.at[src, 2], sp, beside).wait_recv()
+            remote(here, here, r_send, r_recv.at[src, 1], sp, beside).wait_recv()
         total = both(src, tp, slice(0, cap))
         total = total + rrecv[src, 0].astype(F32) + rrecv[src, 1].astype(F32)
 
@@ -1030,10 +1026,10 @@
             pltpu.VMEM((8, toks), F32),
             pltpu.VMEM((tps, 8, toks), F32),
             dma((10,)), dma((3,)),
-            dma, dma, dma, dma((zs, 6)), dma((zs,)),
-            dma, dma((zs, 2)), dma, dma((zs, 3)),
+            dma, dma, dma, dma((zs, 4)), dma((zs,)),
+            dma, dma((zs, 2)), dma, dma((zs, 2)),
             dma, dma, dma, dma((5,)),
-            dma((n,)), dma((n,)), dma((n,)),
+            dma((zs,)), dma((zs,)), dma((n,)),
             dma, dma, dma, dma((n,)),
             dma, dma((3,)), dma, dma, pltpu.SemaphoreType.REGULAR((2,)),
         ],

time: 118 us -> 118 us (level)
  no operation moved by 1% of the time
where the time goes in v2:
time: 118 us
  Pallas kernels  117 us (99%)
    pallas_call x1, Pallas kernels, paired_shards(): pl.pallas_call(functools.partial(layer_kernel, n, tps, cap, heads, head_w...  117 us

profile of v2, /device:TPU:24, one launch (start us, length us, event | category | flops | bytes accessed | tf_op | source)
XLA Modules:
  0.0 117.8 jit_solution(9236215214429163047)
XLA Ops:
  0.0 116.8 %layer.1 = bf16[256,2048]{1,0:T(8,128)(2,1)S(1)} custom-call(bf16[1024,128]{1,0:T(8,128)(2,1)} %bitcast.10, bf16[1024,128]{1,0:T(8,128)(2,1)} %bitcast.11, bf16[1024,128]{1,0:T(8,128)(2,1)} %bitcast.12, s32[2,256]{1,0:T(2,128)} %bitcast.14, f32[2,256]{1,0:T(2,128)} %bitcast.15, bf16[4096,512]{1,0:T(8,128)(2,1)} %bitcast.9, f32[1,4]{1,0:T(1,128)} %bitcast.16, ...), custom_call_target="tpu_custom_call" | custom-call | tf_op jit(solution)/shard_map/layer/pallas_call | solution.py:982
  116.8 1.0 copy.15

commit v3 on v2

--- a/solution.py
+++ b/solution.py
@@ -753,7 +753,8 @@
             return carry
 
         with SC("ffn_two"):
-            lax.fori_loop(0, tps, two, 0)
+            for j in range(tps):
+                two(j, 0)
 
     cap_halves = (slice(0, half_cap), slice(half_cap, cap))
 

time: 118 us -> 117 us (level)
  no operation moved by 1% of the time
where the time goes in v3:
time: 117 us
  Pallas kernels  116 us (99%)
    pallas_call x1, Pallas kernels, paired_shards(): pl.pallas_call(functools.partial(layer_kernel, n, tps, cap, heads, head_w...  116 us

profile of v3, /device:TPU:24, one launch (start us, length us, event | category | flops | bytes accessed | tf_op | source)
XLA Modules:
  0.0 117.1 jit_solution(5862638990704909038)
XLA Ops:
  0.0 116.2 %layer.1 = bf16[256,2048]{1,0:T(8,128)(2,1)S(1)} custom-call(bf16[1024,128]{1,0:T(8,128)(2,1)} %bitcast.10, bf16[1024,128]{1,0:T(8,128)(2,1)} %bitcast.11, bf16[1024,128]{1,0:T(8,128)(2,1)} %bitcast.12, s32[2,256]{1,0:T(2,128)} %bitcast.14, f32[2,256]{1,0:T(2,128)} %bitcast.15, bf16[4096,512]{1,0:T(8,128)(2,1)} %bitcast.9, f32[1,4]{1,0:T(1,128)} %bitcast.16, ...), custom_call_target="tpu_custom_call" | custom-call | tf_op jit(solution)/shard_map/layer/pallas_call | solution.py:983
  116.2 1.0 copy.15
